TPU v7x, 32 devices: a whole 2x2x4 slice. The times are simulated.
32 devices in a mesh: sp: 4 (over y, x), tp: 8 (over z, core).
Axes of the slice: x: 2, y: 2, z: 4, core: 2. Of those that a mesh axis runs over, the one named last changes fastest.
Arguments:
- queries: bfloat16 [2048, 2048], P('sp', 'tp'), may hold values from -8 to 8
- keys: bfloat16 [2048, 1024], P('sp', 'tp'), may hold values from -8 to 8
- values: bfloat16 [2048, 1024], P('sp', 'tp'), may hold values from -6 to 6
- doc_ids: int32 [2048], P('sp'), may hold values from 0 to 1, never falling along the last dimension, each value on 1 to 1536 neighbouring positions
- sink_logits: float32 [32], P('tp'), may hold values from 3 to 6
- out_weight: bfloat16 [2048, 2048], P('tp'), may hold values from -0.75 to 0.75
- residual: bfloat16 [2048, 2048], P(('sp', 'tp')), may hold values from -6 to 6
- norm_gain: float32 [2048], replicated, may hold values from 0.1 to 1.9
- routes: int32 [2048, 2], P(('sp', 'tp')), may hold values from 0 to 3, all different within a row; in each aligned block of 64 rows (0 to 63, 64 to 127, ...) at most 36 rows name the same one
- route_weights: float32 [2048, 2], P(('sp', 'tp')), may hold values from 0.2 to 1
- gate_weight: bfloat16 [4, 2048, 7168], P('sp', None, 'tp'), may hold values from -0.125 to 0.125
- up_weight: bfloat16 [4, 2048, 7168], P('sp', None, 'tp'), may hold values from -0.125 to 0.125
- down_weight: bfloat16 [4, 7168, 2048], P('sp', 'tp'), may hold values from -0.0625 to 0.0625
Outputs:
- layer_output: bfloat16 [2048, 2048], P(('sp', 'tp'))
Inputs may be any that keep to these rules, and one draw needn't show every extreme that they name: `doc_ids`: never falling along the sequence; each document spans 1 to 1536 positions, one exactly that many. `routes`: each row names 2 different experts. In the rows of one device (aligned blocks of 64 rows) no expert is named by more than 36 rows, a bound that some block reaches.
All inputs are finite; a program needn't handle non-finite values.
Results may differ from a plain program's by a relative error of at most 0.015.
Values may be sent and summed in bfloat16 or wider, within the bound.
A program may use at most 128 MiB of HBM per device.

v0:
```python
import math
import jax
import jax.numpy as jnp
from jax import lax
from jax.sharding import PartitionSpec as P

HEAD_DIM = 64
WINDOW = 128
layer_epsilon = 1e-05
masked_score = -1e30


def passed_along(value, axis, steps):
    count = lax.axis_size(axis)
    first, last = (max(0, -steps), min(count, count - steps))
    return lax.ppermute(value, axis, [(source, source + steps) for source in range(first, last)])


def local(
    queries,
    keys,
    values,
    doc_ids,
    sink_logits,
    out_weight,
    residual,
    norm_gain,
    routes,
    route_weights,
    gate_weight,
    up_weight,
    down_weight,
):
    span_rows = queries.shape[0]
    kv_width = keys.shape[1]
    kv_groups = kv_width // HEAD_DIM
    heads_here = queries.shape[1] // HEAD_DIM
    group_ratio = heads_here // kv_groups
    reach_back = WINDOW - 1
    score_scale = 1.0 / math.sqrt(HEAD_DIM)
    doc_float = (doc_ids + 1).astype(jnp.float32)
    key_value = jnp.concatenate([keys, values], axis=1).astype(jnp.float32)
    tail_pairs, tail_docs = (
        passed_along(key_value[span_rows - reach_back :].astype(jnp.bfloat16), "sp", 1).astype(
            jnp.float32
        ),
        passed_along(doc_float[span_rows - reach_back :].astype(jnp.bfloat16), "sp", 1).astype(
            jnp.float32
        ),
    )
    all_keys = jnp.concatenate([tail_pairs[:, :kv_width].astype(jnp.bfloat16), keys], axis=0)
    all_values = jnp.concatenate([tail_pairs[:, kv_width:].astype(jnp.bfloat16), values], axis=0)
    all_docs = jnp.concatenate([tail_docs, doc_float], axis=0)
    block_rows = min(512, span_rows)
    sink_table = sink_logits.reshape(kv_groups, group_ratio, 1)
    offsets = (
        jnp.arange(block_rows)[:, None] + reach_back - jnp.arange(block_rows + reach_back)[None, :]
    )
    window_mask = (offsets >= 0) & (offsets <= reach_back)
    pieces = []
    for block_index in range(span_rows // block_rows):
        first_row = block_index * block_rows
        query_rows = queries[first_row : first_row + block_rows].reshape(
            block_rows, kv_groups, group_ratio, HEAD_DIM
        )
        key_rows = all_keys[first_row : first_row + block_rows + reach_back].reshape(
            block_rows + reach_back, kv_groups, HEAD_DIM
        )
        value_rows = all_values[first_row : first_row + block_rows + reach_back].reshape(
            block_rows + reach_back, kv_groups, HEAD_DIM
        )
        scores = (
            jnp.einsum("bgrd,sgd->grbs", query_rows, key_rows, preferred_element_type=jnp.float32)
            * score_scale
        )
        same_doc = (
            doc_float[first_row : first_row + block_rows][:, None]
            == all_docs[first_row : first_row + block_rows + reach_back][None, :]
        )
        scores = jnp.where(window_mask & same_doc, scores, masked_score)
        row_max = jnp.maximum(scores.max(-1), sink_table)
        exp_scores = jnp.exp(scores - row_max[..., None])
        denominator = exp_scores.sum(-1) + jnp.exp(sink_table - row_max)
        weighted = jnp.einsum(
            "grbs,sgd->bgrd",
            exp_scores.astype(jnp.bfloat16),
            value_rows,
            preferred_element_type=jnp.float32,
        )
        weighted = weighted / jnp.transpose(denominator, (2, 0, 1))[..., None]
        pieces.append(weighted.astype(jnp.bfloat16).reshape(block_rows, heads_here * HEAD_DIM))
    attended = jnp.concatenate(pieces, axis=0)
    rows_here = attended
    projected = lax.psum_scatter(
        jnp.dot(rows_here, out_weight, preferred_element_type=jnp.float32).astype(jnp.bfloat16),
        "tp",
        scatter_dimension=0,
        tiled=True,
    ).astype(jnp.float32)
    stream = residual.astype(jnp.float32) + projected
    mean_value = stream.mean(-1, keepdims=True)
    centred = stream - mean_value
    variance = (centred * centred).mean(-1, keepdims=True)
    normed = (centred * lax.rsqrt(variance + layer_epsilon) * norm_gain).astype(jnp.bfloat16)
    token_count = residual.shape[0]
    width = residual.shape[1]
    route_count = routes.shape[1]
    expert_count = lax.axis_size("sp") * gate_weight.shape[0]
    capacity = 9 * route_count * token_count // (8 * expert_count)
    flat_routes = routes.reshape(-1)
    one_hot = (flat_routes[:, None] == jnp.arange(expert_count)[None, :]).astype(jnp.int32)
    slot_ids = jnp.sum((jnp.cumsum(one_hot, axis=0) - 1) * one_hot, axis=1)
    destination = flat_routes * capacity + slot_ids
    slot_range = jnp.arange(expert_count * capacity)
    selector = jnp.any(
        slot_range[:, None, None] == destination.reshape(token_count, route_count)[None], axis=2
    )
    dispatch = jnp.dot(
        selector.astype(jnp.bfloat16), normed, preferred_element_type=jnp.float32
    ).astype(jnp.bfloat16)
    inbound = lax.all_to_all(
        dispatch.reshape(expert_count, capacity, width),
        "sp",
        split_axis=0,
        concat_axis=0,
        tiled=True,
    )
    arrived = inbound.reshape(-1, width)
    row_piece = lax.all_gather(arrived, "tp", axis=0, tiled=True)
    gate = jnp.dot(row_piece, gate_weight[0], preferred_element_type=jnp.float32)
    upward = jnp.dot(row_piece, up_weight[0], preferred_element_type=jnp.float32)
    hidden = (jax.nn.silu(gate) * upward).astype(jnp.bfloat16)
    rows_here = hidden
    partial_value = jnp.dot(rows_here, down_weight[0], preferred_element_type=jnp.float32).astype(
        jnp.bfloat16
    )
    returned = lax.psum_scatter(
        lax.optimization_barrier(partial_value).astype(jnp.float32).astype(jnp.bfloat16),
        "tp",
        scatter_dimension=0,
        tiled=True,
    )
    back_rows = lax.all_to_all(
        returned.reshape(inbound.shape), "sp", split_axis=0, concat_axis=0, tiled=True
    ).reshape(-1, width)
    picked = back_rows[destination].astype(jnp.float32).reshape(token_count, route_count, width)
    combined = jnp.sum(picked * route_weights[..., None], axis=1)
    return (stream + combined).astype(jnp.bfloat16)


def solution(mesh):
    placed = (
        P("sp", "tp"),
        P("sp", "tp"),
        P("sp", "tp"),
        P("sp"),
        P("tp"),
        P("tp", None),
        P(("sp", "tp"), None),
        P(),
        P(("sp", "tp"), None),
        P(("sp", "tp"), None),
        P("sp", None, "tp"),
        P("sp", None, "tp"),
        P("sp", "tp", None),
    )
    return jax.shard_map(
        local, mesh=mesh, in_specs=placed, out_specs=P(("sp", "tp"), None), check_vma=False
    )
```

profile of v0, /device:TPU:0, one launch (start us, length us, event | category | flops | bytes accessed | tf_op | source)
XLA Modules:
  0.0 232.7 jit_solution(13959658188333084272)
XLA Ops:
  6.5 0.8 fusion.35
  7.3 0.1 slice.18
  7.4 4.9 %collective-permute-start.1 = (bf16[127]{0:T(256)(128)(2,1)S(1)}, bf16[127]{0:T(256)(128)(2,1)S(1)}, u32[]{:S(2)}, u32[]{:S(2)}) collective-permute-start(bf16[127]{0:T(256)(128)(2,1)S(1)} %slice.18), channel_id=1, source_target_pairs={{0,8},{8,16},{16,24},{1,9},{9,17},{17,25},{2,10},{10,18},{18,26},{... | collective-permute-start | bytes 770 | tf_op jit(solution)/shard_map/ppermute | solution.py:16
  12.3 0.8 pad_maximum_fusion.2
  13.1 3.4 %collective-permute-start = (bf16[127,256]{1,0:T(8,128)(2,1)S(1)}, bf16[127,256]{1,0:T(8,128)(2,1)S(1)}, u32[]{:S(2)}, u32[]{:S(2)}) collective-permute-start(bf16[127,256]{1,0:T(8,128)(2,1)S(1)} %pad_maximum_fusion.2), channel_id=1, source_target_pairs={{0,8},{8,16},{16,24},{1,9},{9,17},{17,25},{2,10},{10,18},{18,26},{... | collective-permute-start | bytes 195080 | tf_op jit(solution)/shard_map/ppermute | solution.py:16
  16.5 1.1 copy.30
  17.6 0.7 max.16
  18.3 0.1 pad_maximum_fusion.3
  18.4 0.5 fusion.16
  18.9 1.0 pad_maximum_fusion
  19.9 0.2 copy.29
  20.1 1.1 fusion.2
  21.3 2.2 copy-done.1
  23.5 1.1 fusion
  24.6 0.1 add_bitcast_fusion
  24.7 0.2 copy.28
  24.9 4.0 %fusion.23 = bf16[512,2,2,64]{0,3,2,1:T(8,128)(2,1)S(1)} fusion(bf16[639,2,64,1]{0,2,3,1:T(8,128)(2,1)S(1)} %bitcast.63, f32[2,639,512,2]{2,1,3,0:T(8,128)} %copy-done.1, f32[2,2,512]{2,1,0:T(2,128)S(1)} %broadcast_maximum_fusion, pred[512,639]{0,1:T(8,128)(4,1)S(1)} %fusion.16, f32[512,2,2]{0,2,1:T(2,128)S(1)} %add_bitcast_fusion), kind=kOutput, calls=%fused_computation.25 | convolution fusion | flops 173006848 | bytes 6003968 | tf_op jit(solution)/shard_map/grbs,sgd->bgrd/dot_general | solution.py:84
  28.9 2.1 convolution_convert_fusion.1
  31.1 0.1 copy.32
  31.2 0.1 eq.45
  31.3 0.1 fusion.31
  31.4 0.2 reduce_window_sum.11
  31.6 0.2 select_reduce_fusion
  31.8 0.1 reduce_sum.51
  32.0 0.1 fusion.30
  32.1 36.7 %reduce-scatter.3.cloned.1.call-done = bf16[64,2048]{1,0:T(8,128)(2,1)} async-done(((bf16[512,2048]{1,0:T(8,128)(2,1)}), bf16[64,2048]{1,0:T(8,128)(2,1)}) %reduce-scatter.3.cloned.1.call-update) | async-done | bytes 262160 | tf_op jit(solution)/shard_map/reduce_scatter | solution.py:94
  68.8 1.1 fusion.26
  70.0 1.2 multiply_reduce_fusion.1
  71.2 1.3 convolution_convert_fusion.2
  72.5 0.1 reshape.95
  72.7 11.1 %all_to_all.10 = bf16[4,36,2048]{2,1,0:T(8,128)(2,1)S(1)} all-to-all(bf16[4,36,2048]{2,1,0:T(8,128)(2,1)S(1)} %reshape.95), channel_id=1, replica_groups=mesh['sp'=4,'tp'=8] {'sp'}, dimensions={0} | all-to-all | bytes 1179648 | tf_op jit(solution)/shard_map/all_to_all | solution.py:121
  83.8 1.0 reshape.96
  84.7 0.2 reduce-scatter.5.cloned.1.call-start
  85.0 49.7 %all-gather.2.cloned.1.call-done = bf16[1152,2048]{1,0:T(8,128)(2,1)} async-done(((bf16[144,2048]{1,0:T(8,128)(2,1)}), bf16[1152,2048]{1,0:T(8,128)(2,1)}) %all-gather.2.cloned.1.call-update) | async-done | bytes 4718608 | tf_op jit(solution)/shard_map/all_gather | solution.py:129
  134.7 8.1 %fusion.5 = f32[1152,896]{1,0:T(8,128)S(1)} fusion(bf16[1152,2048]{1,0:T(8,128)(2,1)} %all-gather.2.cloned.1.call-done, bf16[1,2048,896]{2,1,0:T(8,128)(2,1)} %param.23), kind=kOutput, calls=%fused_computation.10 | convolution fusion | flops 4227858432 | bytes 12517376 | tf_op jit(solution)/shard_map/dot_general | solution.py:130
  142.8 5.3 %fusion.7 = bf16[1152,896]{1,0:T(8,128)(2,1)S(1)} fusion(bf16[1152,2048]{1,0:T(8,128)(2,1)S(1)} %copy-done.7, bf16[1,2048,896]{2,1,0:T(8,128)(2,1)S(1)} %copy-done.8, f32[1152,896]{1,0:T(8,128)S(1)} %fusion.5), kind=kOutput, calls=%fused_computation.12 | convolution fusion | flops 4234051584 | bytes 14581760 | tf_op jit(solution)/shard_map/dot_general | solution.py:131
  148.2 6.7 %convolution_convert_fusion = bf16[1152,2048]{1,0:T(8,128)(2,1)} fusion(bf16[1152,896]{1,0:T(8,128)(2,1)S(1)} %fusion.7, bf16[1,896,2048]{2,1,0:T(8,128)(2,1)S(1)} %copy-done.9), kind=kOutput, calls=%fused_computation.1 | convolution fusion | flops 4230217728 | bytes 10452992 | tf_op jit(solution)/shard_map/dot_general | solution.py:134
  154.9 53.8 %reduce-scatter.5.cloned.1.call-done = bf16[144,2048]{1,0:T(8,128)(2,1)} async-done(((bf16[1152,2048]{1,0:T(8,128)(2,1)}), bf16[144,2048]{1,0:T(8,128)(2,1)}) %reduce-scatter.5.cloned.1.call-update) | async-done | bytes 589840 | tf_op jit(solution)/shard_map/reduce_scatter | solution.py:137
  208.7 2.0 reshape.97
  210.7 3.6 %all-to-all-start.1 = ((bf16[4,36,2048]{2,1,0:T(8,128)(2,1)}), bf16[4,36,2048]{2,1,0:T(8,128)(2,1)S(1)}, u32[]{:S(2)}, u32[]{:S(2)}) async-start(bf16[4,36,2048]{2,1,0:T(8,128)(2,1)} %reshape.97), calls=%async_computation.3 | async-start | bytes 1310720 | tf_op jit(solution)/shard_map/all_to_all | solution.py:143
  214.4 0.1 mul.77
  214.5 0.1 copy.35
  214.6 7.4 %all-to-all-done.1 = bf16[4,36,2048]{2,1,0:T(8,128)(2,1)S(1)} async-done(((bf16[4,36,2048]{2,1,0:T(8,128)(2,1)}), bf16[4,36,2048]{2,1,0:T(8,128)(2,1)S(1)}, u32[]{:S(2)}, u32[]{:S(2)}) %all-to-all-start.1) | async-done | bytes 589856 | tf_op jit(solution)/shard_map/all_to_all | solution.py:143
  222.1 0.1 reshape.98
  222.2 0.9 gather_fusion
  223.1 0.7 reshape.99
  223.8 1.5 multiply_reduce_fusion
  225.3 0.8 add_convert_fusion
  (36 shorter events, 0.3 us)
Async XLA Ops:
  6.5 22.4 %copy-start = (bf16[256,2048]{1,0:T(8,128)(2,1)S(1)}, bf16[256,2048]{1,0:T(8,128)(2,1)}, u32[]{:S(2)}) copy-start(bf16[256,2048]{1,0:T(8,128)(2,1)} %param.18) | copy-start | bytes 3145732
  6.5 62.3 %reduce-scatter.3.cloned.1.call-start = ((), (), s32[]{:S(2)}) async-start(), calls=%async_computation.4 | async-start | bytes 2359296 | tf_op jit(solution)/shard_map/reduce_scatter | solution.py:94
  7.4 10.9 %collective-permute-start.1 = (bf16[127]{0:T(256)(128)(2,1)S(1)}, bf16[127]{0:T(256)(128)(2,1)S(1)}, u32[]{:S(2)}, u32[]{:S(2)}) collective-permute-start(bf16[127]{0:T(256)(128)(2,1)S(1)} %slice.18), channel_id=1, source_target_pairs={{0,8},{8,16},{16,24},{1,9},{9,17},{17,25},{2,10},{10,18},{18,26},{... | collective-permute-start | bytes 770 | tf_op jit(solution)/shard_map/ppermute | solution.py:16
  13.1 5.8 %collective-permute-start = (bf16[127,256]{1,0:T(8,128)(2,1)S(1)}, bf16[127,256]{1,0:T(8,128)(2,1)S(1)}, u32[]{:S(2)}, u32[]{:S(2)}) collective-permute-start(bf16[127,256]{1,0:T(8,128)(2,1)S(1)} %pad_maximum_fusion.2), channel_id=1, source_target_pairs={{0,8},{8,16},{16,24},{1,9},{9,17},{17,25},{2,10},{10,18},{18,26},{... | collective-permute-start | bytes 195080 | tf_op jit(solution)/shard_map/ppermute | solution.py:16
  21.2 2.3 copy-start.1
  28.9 2.2 copy-start.5
  28.9 40.0 %copy-start.2 = (bf16[64,2048]{1,0:T(8,128)(2,1)S(1)}, bf16[64,2048]{1,0:T(8,128)(2,1)}, u32[]{:S(2)}) copy-start(bf16[64,2048]{1,0:T(8,128)(2,1)} %param.19) | copy-start | bytes 786436
  28.9 42.3 %copy-start.4 = (f32[2048]{0:T(1024)S(1)}, f32[2048]{0:T(1024)}, u32[]{:S(2)}) copy-start(f32[2048]{0:T(1024)} %param.20) | copy-start | bytes 24580
  31.0 103.7 %all-gather.2.cloned.1.call-start = ((), (), s32[]{:S(2)}) async-start(), calls=%async_computation.5 | async-start | bytes 5308416 | tf_op jit(solution)/shard_map/all_gather | solution.py:129
  84.7 124.0 %reduce-scatter.5.cloned.1.call-start = ((), (), s32[]{:S(2)}) async-start(), calls=%async_computation.6 | async-start | bytes 5308416 | tf_op jit(solution)/shard_map/reduce_scatter | solution.py:137
  134.7 8.1 %copy-start.7 = (bf16[1152,2048]{1,0:T(8,128)(2,1)S(1)}, bf16[1152,2048]{1,0:T(8,128)(2,1)}, u32[]{:S(2)}) copy-start(bf16[1152,2048]{1,0:T(8,128)(2,1)} %all-gather.2.cloned.1.call-done) | copy-start | bytes 14155780
  134.7 8.1 %copy-start.8 = (bf16[1,2048,896]{2,1,0:T(8,128)(2,1)S(1)}, bf16[1,2048,896]{2,1,0:T(8,128)(2,1)}, u32[]{:S(2)}) copy-start(bf16[1,2048,896]{2,1,0:T(8,128)(2,1)} %param.24) | copy-start | bytes 11010052
  142.8 5.3 %copy-start.9 = (bf16[1,896,2048]{2,1,0:T(8,128)(2,1)S(1)}, bf16[1,896,2048]{2,1,0:T(8,128)(2,1)}, u32[]{:S(2)}) copy-start(bf16[1,896,2048]{2,1,0:T(8,128)(2,1)} %param.25) | copy-start | bytes 11010052
  154.9 59.6 %copy-start.6 = (f32[64,2]{0,1:T(2,128)S(1)}, f32[64,2]{0,1:T(2,128)}, u32[]{:S(2)}) copy-start(f32[64,2]{0,1:T(2,128)} %param.22) | copy-start | bytes 1540
  210.7 11.3 %all-to-all-start.1 = ((bf16[4,36,2048]{2,1,0:T(8,128)(2,1)}), bf16[4,36,2048]{2,1,0:T(8,128)(2,1)S(1)}, u32[]{:S(2)}, u32[]{:S(2)}) async-start(bf16[4,36,2048]{2,1,0:T(8,128)(2,1)} %reshape.97), calls=%async_computation.3 | async-start | bytes 1310720 | tf_op jit(solution)/shard_map/all_to_all | solution.py:143
  222.2 3.2 %copy-start.3 = (bf16[64,2048]{1,0:T(8,128)(2,1)S(1)}, bf16[64,2048]{1,0:T(8,128)(2,1)}, u32[]{:S(2)}) copy-start(bf16[64,2048]{1,0:T(8,128)(2,1)} %reduce-scatter.3.cloned.1.call-done) | copy-start | bytes 786436
Sparse Core Ops, SparseCore 0:
  31.1 37.6 reduce-scatter.2
  84.9 49.7 all-gather.1
  155.0 53.6 reduce-scatter.4
where the time goes:
time: 233 us
  waiting for transfers between devices  148 us (64%)
  matrix products  28.7 us (12%)
  between operations  13.4 us (6%)
  starting transfers between devices  12.2 us (5%)
  blocking collectives  11.1 us (5%)
  local copies, waits for them, and re-layouts  9.98 us (4%)
  other arithmetic  9.64 us (4%)
    reduce_scatter x1, waiting for transfers between devices, local(): lax.psum_scatter(lax.optimization_barrier(partial_value).astype(jnp.float...  53.8 us
    all_gather x1, waiting for transfers between devices, local(): row_piece = lax.all_gather(arrived, 'tp', axis=0, tiled=True)  49.7 us
    reduce_scatter x1, waiting for transfers between devices, local(): lax.psum_scatter(jnp.dot(rows_here, out_weight, preferred_element_type=jn...  36.7 us
    all_to_all x1, blocking collectives, local(): lax.all_to_all(dispatch.reshape(expert_count, capacity, width), 'sp', spl...  11.1 us
    ppermute x2, starting transfers between devices, passed_along(): lax.ppermute(value, axis, [(source, source + steps) for source in range(f...  8.26 us
    dot_general x1, matrix products, local(): jnp.dot(row_piece, gate_weight[0], preferred_element_type=jnp.float32)  8.11 us
    all_to_all x1, waiting for transfers between devices, local(): lax.all_to_all(returned.reshape(inbound.shape), 'sp', split_axis=0, conca...  7.42 us
    dot_general x1, matrix products, local(): jnp.dot(rows_here, down_weight[0], preferred_element_type=jnp.float32)  6.73 us
  transfers between devices with their start and end apart: 6, of which 4 were waited for; matrix products, arithmetic and copies ran while one was open for 2% of the time, Pallas kernels for 0%

commit v1 on v0

--- a/solution.py
+++ b/solution.py
@@ -126,7 +126,9 @@
         tiled=True,
     )
     arrived = inbound.reshape(-1, width)
-    row_piece = lax.all_gather(arrived, "tp", axis=0, tiled=True)
+    row_piece = jnp.concatenate(
+        lax.all_to_all(jnp.stack([arrived] * lax.axis_size("tp")), "tp", 0, 0), axis=0
+    )
     gate = jnp.dot(row_piece, gate_weight[0], preferred_element_type=jnp.float32)
     upward = jnp.dot(row_piece, up_weight[0], preferred_element_type=jnp.float32)
     hidden = (jax.nn.silu(gate) * upward).astype(jnp.bfloat16)

time: 233 us -> 288 us (1.24)
  blocking collectives: 11.1 us -> 120 us
  waiting for transfers between devices: 148 us -> 96.6 us
  matrix products: 28.7 us -> 25.6 us
    all_to_all x0 -> x1, blocking collectives: none -> 109 us  [local(): lax.all_to_all(jnp.stack([arrived] * lax.axis_size('tp')), 'tp', 0, 0)]
    all_gather x1 -> x0, waiting for transfers between devices: 49.7 us -> none  [local(): row_piece = lax.all_gather(arrived, 'tp', axis=0, tiled=True)]
    dot_general x1, matrix products: 8.11 us -> 5.09 us  [local(): jnp.dot(row_piece, gate_weight[0], preferred_element_type=jnp.float32)]
  transfers between devices with their start and end apart: 6 -> 5, of which waited for: 4 -> 3; matrix products, arithmetic and copies ran while one was open for 2% -> 2% of each run, Pallas kernels for 0% -> 0%
where the time goes in v1:
time: 288 us; the launch traced here: 287 us
  blocking collectives  120 us (42%)
  waiting for transfers between devices  96.6 us (34%)
  matrix products  25.6 us (9%)
  between operations  13.7 us (5%)
  starting transfers between devices  12 us (4%)
  local copies, waits for them, and re-layouts  9.74 us (3%)
  other arithmetic  9.64 us (3%)
    all_to_all x1, blocking collectives, local(): lax.all_to_all(jnp.stack([arrived] * lax.axis_size('tp')), 'tp', 0, 0)  109 us
    reduce_scatter x1, waiting for transfers between devices, local(): lax.psum_scatter(lax.optimization_barrier(partial_value).astype(jnp.float...  52.4 us
    reduce_scatter x1, waiting for transfers between devices, local(): lax.psum_scatter(jnp.dot(rows_here, out_weight, preferred_element_type=jn...  36.7 us
    all_to_all x1, blocking collectives, local(): lax.all_to_all(dispatch.reshape(expert_count, capacity, width), 'sp', spl...  11.1 us
    ppermute x2, starting transfers between devices, passed_along(): lax.ppermute(value, axis, [(source, source + steps) for source in range(f...  8.26 us
    all_to_all x1, waiting for transfers between devices, local(): lax.all_to_all(returned.reshape(inbound.shape), 'sp', split_axis=0, conca...  7.41 us
    dot_general x1, matrix products, local(): jnp.dot(rows_here, down_weight[0], preferred_element_type=jnp.float32)  6.73 us
  transfers between devices with their start and end apart: 5, of which 3 were waited for; matrix products, arithmetic and copies ran while one was open for 2% of the time, Pallas kernels for 0%

profile of v1, /device:TPU:0, one launch (start us, length us, event | category | flops | bytes accessed | tf_op | source)
XLA Modules:
  0.0 287.4 jit_solution(17932901524983826513)
XLA Ops:
  6.5 0.8 fusion.35
  7.3 0.1 slice.18
  7.4 4.9 %collective-permute-start.1 = (bf16[127]{0:T(256)(128)(2,1)S(1)}, bf16[127]{0:T(256)(128)(2,1)S(1)}, u32[]{:S(2)}, u32[]{:S(2)}) collective-permute-start(bf16[127]{0:T(256)(128)(2,1)S(1)} %slice.18), channel_id=1, source_target_pairs={{0,8},{8,16},{16,24},{1,9},{9,17},{17,25},{2,10},{10,18},{18,26},{... | collective-permute-start | bytes 770 | tf_op jit(solution)/shard_map/ppermute | solution.py:16
  12.3 0.8 pad_maximum_fusion.2
  13.1 3.4 %collective-permute-start = (bf16[127,256]{1,0:T(8,128)(2,1)S(1)}, bf16[127,256]{1,0:T(8,128)(2,1)S(1)}, u32[]{:S(2)}, u32[]{:S(2)}) collective-permute-start(bf16[127,256]{1,0:T(8,128)(2,1)S(1)} %pad_maximum_fusion.2), channel_id=1, source_target_pairs={{0,8},{8,16},{16,24},{1,9},{9,17},{17,25},{2,10},{10,18},{18,26},{... | collective-permute-start | bytes 195080 | tf_op jit(solution)/shard_map/ppermute | solution.py:16
  16.5 1.1 copy.30
  17.6 0.7 max.16
  18.3 0.1 pad_maximum_fusion.3
  18.4 0.5 fusion.16
  18.9 1.0 pad_maximum_fusion
  19.9 0.2 copy.29
  20.1 1.1 fusion.2
  21.3 2.2 copy-done.1
  23.5 1.1 fusion
  24.6 0.1 add_bitcast_fusion
  24.7 0.2 copy.28
  24.9 4.0 %fusion.23 = bf16[512,2,2,64]{0,3,2,1:T(8,128)(2,1)S(1)} fusion(bf16[639,2,64,1]{0,2,3,1:T(8,128)(2,1)S(1)} %bitcast.66, f32[2,639,512,2]{2,1,3,0:T(8,128)} %copy-done.1, f32[2,2,512]{2,1,0:T(2,128)S(1)} %broadcast_maximum_fusion, pred[512,639]{0,1:T(8,128)(4,1)S(1)} %fusion.16, f32[512,2,2]{0,2,1:T(2,128)S(1)} %add_bitcast_fusion), kind=kOutput, calls=%fused_computation.25 | convolution fusion | flops 173006848 | bytes 6003968 | tf_op jit(solution)/shard_map/grbs,sgd->bgrd/dot_general | solution.py:84
  28.9 2.1 convolution_convert_fusion.1
  31.1 0.1 copy.32
  31.2 0.1 eq.45
  31.3 0.1 fusion.31
  31.4 0.2 reduce_window_sum.11
  31.6 0.2 select_reduce_fusion
  31.8 0.1 reduce_sum.51
  32.0 0.1 fusion.30
  32.1 36.7 %reduce-scatter.3.cloned.1.call-done = bf16[64,2048]{1,0:T(8,128)(2,1)} async-done(((bf16[512,2048]{1,0:T(8,128)(2,1)}), bf16[64,2048]{1,0:T(8,128)(2,1)}) %reduce-scatter.3.cloned.1.call-update) | async-done | bytes 262160 | tf_op jit(solution)/shard_map/reduce_scatter | solution.py:94
  68.8 1.1 fusion.26
  70.0 1.2 multiply_reduce_fusion.1
  71.2 1.3 convolution_convert_fusion.2
  72.5 0.1 reshape.97
  72.7 11.1 %all_to_all.15 = bf16[4,36,2048]{2,1,0:T(8,128)(2,1)S(1)} all-to-all(bf16[4,36,2048]{2,1,0:T(8,128)(2,1)S(1)} %reshape.97), channel_id=1, replica_groups=mesh['sp'=4,'tp'=8] {'sp'}, dimensions={0} | all-to-all | bytes 1179648 | tf_op jit(solution)/shard_map/all_to_all | solution.py:121
  83.8 0.1 stack_reshape.2
  83.9 0.6 stack.3
  84.5 109.0 %all_to_all.16 = bf16[8,144,2048]{2,1,0:T(8,128)(2,1)S(1)} all-to-all(bf16[8,144,2048]{2,1,0:T(8,128)(2,1)S(1)} %stack.3), channel_id=1, replica_groups=mesh['sp'=4,'tp'=8] {'tp'}, dimensions={0} | all-to-all | bytes 9437184 | tf_op jit(solution)/shard_map/all_to_all | solution.py:130
  193.5 5.1 %fusion.5 = f32[1152,896]{1,0:T(8,128)S(1)} fusion(bf16[1152,2048]{1,0:T(8,128)(2,1)S(1)} %bitcast.62, bf16[1,2048,896]{2,1,0:T(8,128)(2,1)S(1)} %copy-done.7), kind=kOutput, calls=%fused_computation.10 | convolution fusion | flops 4227858432 | bytes 12517376 | tf_op jit(solution)/shard_map/dot_general | solution.py:132
  198.6 5.3 %fusion.7 = bf16[1152,896]{1,0:T(8,128)(2,1)S(1)} fusion(bf16[1152,2048]{1,0:T(8,128)(2,1)S(1)} %bitcast.63, bf16[1,2048,896]{2,1,0:T(8,128)(2,1)S(1)} %copy-done.8, f32[1152,896]{1,0:T(8,128)S(1)} %fusion.5), kind=kOutput, calls=%fused_computation.12 | convolution fusion | flops 4234051584 | bytes 14581760 | tf_op jit(solution)/shard_map/dot_general | solution.py:133
  203.9 6.7 %convolution_convert_fusion = bf16[1152,2048]{1,0:T(8,128)(2,1)} fusion(bf16[1152,896]{1,0:T(8,128)(2,1)S(1)} %fusion.7, bf16[1,896,2048]{2,1,0:T(8,128)(2,1)S(1)} %copy-done.9), kind=kOutput, calls=%fused_computation.1 | convolution fusion | flops 4230217728 | bytes 10452992 | tf_op jit(solution)/shard_map/dot_general | solution.py:136
  210.7 52.4 %reduce-scatter.5.cloned.1.call-done = bf16[144,2048]{1,0:T(8,128)(2,1)} async-done(((bf16[1152,2048]{1,0:T(8,128)(2,1)}), bf16[144,2048]{1,0:T(8,128)(2,1)}) %reduce-scatter.5.cloned.1.call-update) | async-done | bytes 589840 | tf_op jit(solution)/shard_map/reduce_scatter | solution.py:139
  263.1 2.0 reshape.99
  265.1 3.6 %all-to-all-start.2 = ((bf16[4,36,2048]{2,1,0:T(8,128)(2,1)}), bf16[4,36,2048]{2,1,0:T(8,128)(2,1)S(1)}, u32[]{:S(2)}, u32[]{:S(2)}) async-start(bf16[4,36,2048]{2,1,0:T(8,128)(2,1)} %reshape.99), calls=%async_computation.4 | async-start | bytes 1310720 | tf_op jit(solution)/shard_map/all_to_all | solution.py:145
  268.8 0.1 mul.77
  268.9 0.1 copy.35
  269.0 7.4 %all-to-all-done.2 = bf16[4,36,2048]{2,1,0:T(8,128)(2,1)S(1)} async-done(((bf16[4,36,2048]{2,1,0:T(8,128)(2,1)}), bf16[4,36,2048]{2,1,0:T(8,128)(2,1)S(1)}, u32[]{:S(2)}, u32[]{:S(2)}) %all-to-all-start.2) | async-done | bytes 589856 | tf_op jit(solution)/shard_map/all_to_all | solution.py:145
  276.5 0.1 reshape.100
  276.6 0.9 gather_fusion
  277.5 0.7 reshape.101
  278.2 1.5 multiply_reduce_fusion
  279.7 0.8 add_convert_fusion
  (35 shorter events, 0.3 us)
Async XLA Ops:
  6.5 22.4 %copy-start = (bf16[256,2048]{1,0:T(8,128)(2,1)S(1)}, bf16[256,2048]{1,0:T(8,128)(2,1)}, u32[]{:S(2)}) copy-start(bf16[256,2048]{1,0:T(8,128)(2,1)} %param.18) | copy-start | bytes 3145732
  6.5 62.3 %reduce-scatter.3.cloned.1.call-start = ((), (), s32[]{:S(2)}) async-start(), calls=%async_computation.5 | async-start | bytes 2359296 | tf_op jit(solution)/shard_map/reduce_scatter | solution.py:94
  7.4 10.9 %collective-permute-start.1 = (bf16[127]{0:T(256)(128)(2,1)S(1)}, bf16[127]{0:T(256)(128)(2,1)S(1)}, u32[]{:S(2)}, u32[]{:S(2)}) collective-permute-start(bf16[127]{0:T(256)(128)(2,1)S(1)} %slice.18), channel_id=1, source_target_pairs={{0,8},{8,16},{16,24},{1,9},{9,17},{17,25},{2,10},{10,18},{18,26},{... | collective-permute-start | bytes 770 | tf_op jit(solution)/shard_map/ppermute | solution.py:16
  13.1 5.8 %collective-permute-start = (bf16[127,256]{1,0:T(8,128)(2,1)S(1)}, bf16[127,256]{1,0:T(8,128)(2,1)S(1)}, u32[]{:S(2)}, u32[]{:S(2)}) collective-permute-start(bf16[127,256]{1,0:T(8,128)(2,1)S(1)} %pad_maximum_fusion.2), channel_id=1, source_target_pairs={{0,8},{8,16},{16,24},{1,9},{9,17},{17,25},{2,10},{10,18},{18,26},{... | collective-permute-start | bytes 195080 | tf_op jit(solution)/shard_map/ppermute | solution.py:16
  21.2 2.3 copy-start.1
  28.9 2.2 copy-start.5
  28.9 40.0 %copy-start.2 = (bf16[64,2048]{1,0:T(8,128)(2,1)S(1)}, bf16[64,2048]{1,0:T(8,128)(2,1)}, u32[]{:S(2)}) copy-start(bf16[64,2048]{1,0:T(8,128)(2,1)} %param.19) | copy-start | bytes 786436
  28.9 42.3 %copy-start.4 = (f32[2048]{0:T(1024)S(1)}, f32[2048]{0:T(1024)}, u32[]{:S(2)}) copy-start(f32[2048]{0:T(1024)} %param.20) | copy-start | bytes 24580
  31.0 232.1 %reduce-scatter.5.cloned.1.call-start = ((), (), s32[]{:S(2)}) async-start(), calls=%async_computation.6 | async-start | bytes 5308416 | tf_op jit(solution)/shard_map/reduce_scatter | solution.py:139
  84.5 109.0 %copy-start.7 = (bf16[1,2048,896]{2,1,0:T(8,128)(2,1)S(1)}, bf16[1,2048,896]{2,1,0:T(8,128)(2,1)}, u32[]{:S(2)}) copy-start(bf16[1,2048,896]{2,1,0:T(8,128)(2,1)} %param.23) | copy-start | bytes 11010052
  193.5 5.1 %copy-start.8 = (bf16[1,2048,896]{2,1,0:T(8,128)(2,1)S(1)}, bf16[1,2048,896]{2,1,0:T(8,128)(2,1)}, u32[]{:S(2)}) copy-start(bf16[1,2048,896]{2,1,0:T(8,128)(2,1)} %param.24) | copy-start | bytes 11010052
  198.6 5.3 %copy-start.9 = (bf16[1,896,2048]{2,1,0:T(8,128)(2,1)S(1)}, bf16[1,896,2048]{2,1,0:T(8,128)(2,1)}, u32[]{:S(2)}) copy-start(bf16[1,896,2048]{2,1,0:T(8,128)(2,1)} %param.25) | copy-start | bytes 11010052
  210.7 58.3 %copy-start.6 = (f32[64,2]{0,1:T(2,128)S(1)}, f32[64,2]{0,1:T(2,128)}, u32[]{:S(2)}) copy-start(f32[64,2]{0,1:T(2,128)} %param.22) | copy-start | bytes 1540
  265.1 11.3 %all-to-all-start.2 = ((bf16[4,36,2048]{2,1,0:T(8,128)(2,1)}), bf16[4,36,2048]{2,1,0:T(8,128)(2,1)S(1)}, u32[]{:S(2)}, u32[]{:S(2)}) async-start(bf16[4,36,2048]{2,1,0:T(8,128)(2,1)} %reshape.99), calls=%async_computation.4 | async-start | bytes 1310720 | tf_op jit(solution)/shard_map/all_to_all | solution.py:145
  276.6 3.2 %copy-start.3 = (bf16[64,2048]{1,0:T(8,128)(2,1)S(1)}, bf16[64,2048]{1,0:T(8,128)(2,1)}, u32[]{:S(2)}) copy-start(bf16[64,2048]{1,0:T(8,128)(2,1)} %reduce-scatter.3.cloned.1.call-done) | copy-start | bytes 786436
Sparse Core Ops, SparseCore 0:
  31.1 37.6 reduce-scatter.2
  210.8 52.2 reduce-scatter.4
